TPU v7x, 32 devices: a whole 2x2x4 slice. The times are simulated.
32 devices in a mesh: grp: 2 (over y), ep: 8 (over z, core), tp: 2 (over x).
Axes of the slice: x: 2, y: 2, z: 4, core: 2. Of those that a mesh axis runs over, the one named last changes fastest.
Arguments:
- tokens: bfloat16 [2048, 4096], P(('grp', 'ep'), 'tp'), parts along dimension 0, may hold values from -6 to 6
- routes: int32 [2048, 4], P(('grp', 'ep')), parts along dimension 0, may hold values from 0 to 7, all different within a row; in each aligned block of 128 rows (0 to 127, 128 to 255, ...) at most 128 rows name the same one
- route_weights: float32 [2048, 4], P(('grp', 'ep')), parts along dimension 0, may hold values from 0.1 to 1
- norm_gain: float32 [4096], replicated, may hold values from 0.1 to 1.9
- expert_gate: bfloat16 [8, 4096, 1024], P('ep', 'tp'), may hold values from -0.09375 to 0.09375
- expert_up: bfloat16 [8, 4096, 1024], P('ep', 'tp'), may hold values from -0.09375 to 0.09375
- expert_down: bfloat16 [8, 1024, 4096], P('ep', None, 'tp')
- shared_gate: bfloat16 [4096, 1024], P('tp'), may hold values from -0.09375 to 0.09375
- shared_up: bfloat16 [4096, 1024], P('tp'), may hold values from -0.09375 to 0.09375
- shared_down: bfloat16 [1024, 4096], P(None, 'tp')
- out_gain: float32 [4096], P('tp'), may hold values from 0.1 to 1.9
Outputs:
- layer_out: bfloat16 [2048, 4096], P(('grp', 'ep'), 'tp'), parts along dimension 0
There are 2 independent parts, one for each index of `grp`. A program takes and returns all parts, laid end to end along the dimension named above; an argument that names none is the same for every part. Nothing has to cross between parts.
Inputs may be any that keep to these rules, and one draw needn't show every extreme that they name: `routes`: each row names 4 different experts; among the rows of one index of ep no expert is named more than 128 times, and in some such block some expert is named exactly 128 times.
All inputs are finite; a program needn't handle non-finite values.
Results may differ from a plain program's by a relative error of at most 0.023.
Values may be sent and summed in bfloat16 or wider, within the bound.
A program may use at most 64 MiB of HBM per device.

v0:
```python
import jax
import jax.numpy as jnp
from jax import lax
from jax.sharding import PartitionSpec as P

epsilon = 1e-06


def local_product(source, matrix):
    return jnp.dot(source, matrix, preferred_element_type=jnp.float32)


def per_device(
    tokens,
    routes,
    route_weights,
    norm_gain,
    expert_gate,
    expert_up,
    expert_down,
    shared_gate,
    shared_up,
    shared_down,
    out_gain,
):
    block_width = tokens.shape[1]
    full_width = block_width * lax.axis_size("tp")
    width_index = lax.axis_index("tp")
    full_rows = lax.all_gather(tokens, "tp", axis=1, tiled=True)
    full_float = full_rows.astype(jnp.float32)
    normed_full = (
        full_float
        * lax.rsqrt(jnp.mean(full_float * full_float, axis=-1, keepdims=True) + epsilon)
        * norm_gain
    ).astype(jnp.bfloat16)
    normed_block = lax.dynamic_slice_in_dim(normed_full, width_index * block_width, block_width, 1)
    gate_matrix = expert_gate[0]
    up_matrix = expert_up[0]
    down_matrix = expert_down[0]
    experts = lax.axis_size("ep")
    choose = (routes[:, :, None] == jnp.arange(experts, dtype=jnp.int32)[None, None, :]).astype(
        jnp.float32
    )
    weight_table = jnp.sum(route_weights[:, :, None] * choose, axis=1)
    expert_input = lax.all_gather(normed_block, "ep", axis=0, tiled=True)
    table_all = lax.all_gather(weight_table, "ep", axis=0, tiled=True)
    summed = (
        lax.psum(local_product(expert_input, gate_matrix).astype(jnp.bfloat16), "tp").astype(
            jnp.float32
        ),
        lax.psum(local_product(expert_input, up_matrix).astype(jnp.bfloat16), "tp").astype(
            jnp.float32
        ),
        lax.psum(local_product(normed_block, shared_gate).astype(jnp.bfloat16), "tp").astype(
            jnp.float32
        ),
        lax.psum(local_product(normed_block, shared_up).astype(jnp.bfloat16), "tp").astype(
            jnp.float32
        ),
    )
    routed_hidden = (jax.nn.silu(summed[0]) * summed[1]).astype(jnp.bfloat16)
    shared_hidden = (jax.nn.silu(summed[2]) * summed[3]).astype(jnp.bfloat16)
    expert_rows = local_product(routed_hidden, down_matrix).astype(jnp.bfloat16)
    shared_out = local_product(shared_hidden, shared_down)
    own_expert = lax.axis_index("ep")
    column = lax.dynamic_slice_in_dim(table_all, own_expert, 1, 1)
    routed = lax.psum_scatter(
        (column * expert_rows.astype(jnp.float32)).astype(jnp.bfloat16),
        "ep",
        scatter_dimension=0,
        tiled=True,
    ).astype(jnp.float32)
    mixture = routed + shared_out
    square_sum = lax.psum(jnp.sum(mixture * mixture, axis=-1, keepdims=True), "tp")
    scale = lax.rsqrt(square_sum / full_width + epsilon)
    return (mixture * scale * out_gain).astype(jnp.bfloat16)


def solution(mesh):
    return jax.shard_map(
        per_device,
        mesh=mesh,
        in_specs=(
            P(("grp", "ep"), "tp"),
            P(("grp", "ep"), None),
            P(("grp", "ep"), None),
            P(),
            P("ep", "tp", None),
            P("ep", "tp", None),
            P("ep", None, "tp"),
            P("tp", None),
            P("tp", None),
            P(None, "tp"),
            P("tp"),
        ),
        out_specs=P(("grp", "ep"), "tp"),
        check_vma=False,
    )
```

profile of v0, /device:TPU:0, one launch (start us, length us, event | category | flops | bytes accessed | tf_op | source)
XLA Modules:
  0.0 293.4 jit_solution(16838798850096647116)
XLA Ops:
  6.5 0.0 all-gather.3.cloned.1.call-start
  6.5 0.7 all-gather.3.cloned.1.call-update
  7.3 0.0 all-gather.5.cloned.1.call-start
  7.3 0.0 dynamic-slice-start
  7.3 25.6 %all-gather.3.cloned.1.call-done = bf16[128,4096]{1,0:T(8,128)(2,1)} async-done(((bf16[128,2048]{1,0:T(8,128)(2,1)}), bf16[128,4096]{1,0:T(8,128)(2,1)}) %all-gather.3.cloned.1.call-update) | async-done | bytes 1048592 | tf_op jit(solution)/shard_map/all_gather | solution.py:29
  32.9 1.5 multiply_reduce_fusion
  34.4 1.4 convert_element_type.52
  35.9 0.0 dynamic-slice-done
  35.9 1.0 fusion.22
  36.8 0.0 copy-start
  36.8 0.0 all-gather.5.cloned.1.call-update
  36.9 0.0 all-reduce.3.cloned.1.call-start
  36.9 0.0 copy-start.1
  36.9 3.9 %convolution_convert_fusion = bf16[128,1024]{1,0:T(8,128)(2,1)} fusion(bf16[128,2048]{1,0:T(8,128)(2,1)} %fusion.22, bf16[2048,1024]{1,0:T(8,128)(2,1)} %param.19), kind=kOutput, calls=%fused_computation.19 | convolution fusion | flops 537001984 | bytes 4980736 | tf_op jit(solution)/shard_map/dot_general | solution.py:10
  40.8 0.0 copy-done
  40.9 0.0 copy-done.1
  40.9 1.5 convolution_convert_fusion.1
  42.3 41.6 %all-gather.5.cloned.1.call-done = bf16[1024,2048]{1,0:T(8,128)(2,1)} async-done(((bf16[128,2048]{1,0:T(8,128)(2,1)}), bf16[1024,2048]{1,0:T(8,128)(2,1)}) %all-gather.5.cloned.1.call-update) | async-done | bytes 4194320 | tf_op jit(solution)/shard_map/all_gather | solution.py:45
  83.9 0.0 copy-start.5
  83.9 0.0 copy-start.6
  83.9 9.5 %fusion.15 = bf16[1024,1024]{1,0:T(8,128)(2,1)} fusion(bf16[1024,2048]{1,0:T(8,128)(2,1)} %all-gather.5.cloned.1.call-done, bf16[1,2048,1024]{2,1,0:T(8,128)(2,1)} %param.15), kind=kOutput, calls=%fused_computation.17 | convolution fusion | flops 4296015872 | bytes 10485760 | tf_op jit(solution)/shard_map/dot_general | solution.py:10
  93.4 0.0 copy-done.5
  93.4 0.0 copy-done.6
  93.4 5.7 %fusion.18 = bf16[1024,1024]{1,0:T(8,128)(2,1)} fusion(bf16[1024,2048]{1,0:T(8,128)(2,1)S(1)} %copy-done.6, bf16[1,2048,1024]{2,1,0:T(8,128)(2,1)S(1)} %copy-done.5), kind=kOutput, calls=%fused_computation.18 | convolution fusion | flops 4296015872 | bytes 10485760 | tf_op jit(solution)/shard_map/dot_general | solution.py:10
  99.1 0.0 copy-start.3
  99.1 0.0 copy-start.4
  99.1 0.0 all-reduce.3.cloned.1.call-update
  99.1 0.0 reduce-scatter.2.cloned.1.call-start
  99.2 0.6 copy-done.3
  99.8 0.0 copy-done.4
  99.8 14.1 %all_gather.9 = f32[1024,8]{0,1:T(8,128)S(1)} all-gather(f32[128,8]{0,1:T(8,128)S(1)} %select_reduce_fusion), channel_id=1, replica_groups=mesh['grp'=2,'ep'=8,'tp'=2] {'ep'}, dimensions={0}, use_global_device_ids=true | all-gather | bytes 36864 | tf_op jit(solution)/shard_map/all_gather | solution.py:46
  113.9 103.5 %all-reduce.3.cloned.1.call-done = (bf16[1024,1024]{1,0:T(8,128)(2,1)}, bf16[1024,1024]{1,0:T(8,128)(2,1)}, bf16[128,1024]{1,0:T(8,128)(2,1)}, bf16[128,1024]{1,0:T(8,128)(2,1)}) async-done(((bf16[1024,1024]{1,0:T(8,128)(2,1)}, bf16[1024,1024]{1,0:T(8,128)(2,1)}, bf16[128,1024]{1,0:T(8,128)(2,1)}, bf16[128,1024]{1,0:T(8,128)(2,1)}), (bf16[1024,1024]{1,0:T(8,128)(2,1)}, bf16[1024,1024]{1,0:T(8,128)(2,1)}, ...) | async-done | bytes 4718608 | tf_op jit(solution)/shard_map/psum | solution.py:51
  217.4 10.3 %multiply_convert_fusion = bf16[1024,2048]{1,0:T(8,128)(2,1)} fusion(f32[1024]{0:T(1024)S(1)} %bitcast.26, bf16[1,1024,2048]{2,1,0:T(8,128)(2,1)} %param.17, bf16[1024,1024]{1,0:T(8,128)(2,1)} %get-tuple-element.5, bf16[1024,1024]{1,0:T(8,128)(2,1)} %get-tuple-element.6), kind=kOutput, calls=%fused_computation | convolution fusion | flops 4311744512 | bytes 12587008 | tf_op jit(solution)/shard_map/dot_general | solution.py:10
  227.7 0.0 copy-start.7
  227.7 0.0 copy-start.8
  227.7 0.0 reduce-scatter.2.cloned.1.call-update
  227.7 0.0 copy-start.2
  227.7 50.1 %reduce-scatter.2.cloned.1.call-done = bf16[128,2048]{1,0:T(8,128)(2,1)} async-done(((bf16[1024,2048]{1,0:T(8,128)(2,1)}), bf16[128,2048]{1,0:T(8,128)(2,1)}) %reduce-scatter.2.cloned.1.call-update) | async-done | bytes 524304 | tf_op jit(solution)/shard_map/reduce_scatter | solution.py:67
  277.8 0.0 copy-done.7
  277.8 0.0 copy-done.8
  277.8 3.2 %multiply_reduce_fusion.1 = (f32[128]{0:T(128)S(1)}, f32[128,2048]{1,0:T(8,128)S(1)}) fusion(bf16[1024,2048]{1,0:T(8,128)(2,1)} %param.20, bf16[128,1024]{1,0:T(8,128)(2,1)S(1)} %copy-done.7, bf16[128,1024]{1,0:T(8,128)(2,1)S(1)} %copy-done.8, bf16[128,2048]{1,0:T(8,128)(2,1)} %reduce-scatter.2.cloned.1.call-done), kind=kOutput, calls=%fused_computation.25 | convolution fusion | flops 538967936 | bytes 6291968 | tf_op jit(solution)/shard_map/dot_general | solution.py:10
  281.0 4.9 %psum.39 = f32[128,1]{0,1:T(1,128)S(1)} all-reduce(f32[128,1]{0,1:T(1,128)S(1)} %bitcast.27), channel_id=1, replica_groups=mesh['grp'=2,'ep'=8,'tp'=2] {'tp'}, use_global_device_ids=true, to_apply=%region_8.9 | all-reduce | flops 128 | bytes 1024 | tf_op jit(solution)/shard_map/psum | solution.py:74
  285.9 0.0 copy-done.2
  286.0 1.0 multiply_convert_fusion.1
  (4 shorter events, 0.0 us)
Async XLA Ops:
  6.5 26.4 %all-gather.3.cloned.1.call-start = ((), (), s32[]{:S(2)}) async-start(), calls=%async_computation.1 | async-start | bytes 1572864 | tf_op jit(solution)/shard_map/all_gather | solution.py:29
  7.3 76.6 %all-gather.5.cloned.1.call-start = ((), (), s32[]{:S(2)}) async-start(), calls=%async_computation.2 | async-start | bytes 4718592 | tf_op jit(solution)/shard_map/all_gather | solution.py:45
  7.3 28.6 %dynamic-slice-start = ((f32[4096]{0:T(1024)}, s32[]{:T(128)}), f32[2048]{0:T(1024)S(1)}, s32[]{:S(2)}) async-start(f32[4096]{0:T(1024)} %param.14, s32[]{:T(128)} %select_n.7), calls=%async_computation.5 | async-start | bytes 16896 | tf_op jit(solution)/shard_map/dynamic_slice | solution.py:36
  36.8 4.0 %copy-start = (bf16[128,2048]{1,0:T(8,128)(2,1)S(1)}, bf16[128,2048]{1,0:T(8,128)(2,1)}, u32[]{:S(2)}) copy-start(bf16[128,2048]{1,0:T(8,128)(2,1)} %fusion.22) | copy-start | bytes 1572868
  36.9 180.5 %all-reduce.3.cloned.1.call-start = ((), (), s32[]{:S(2)}) async-start(), calls=%async_computation.4 | async-start | bytes 9437184 | tf_op jit(solution)/shard_map/psum | solution.py:51
  36.9 3.9 %copy-start.1 = (bf16[2048,1024]{1,0:T(8,128)(2,1)S(1)}, bf16[2048,1024]{1,0:T(8,128)(2,1)}, u32[]{:S(2)}) copy-start(bf16[2048,1024]{1,0:T(8,128)(2,1)} %param.18) | copy-start | bytes 12582916
  83.9 9.5 %copy-start.5 = (bf16[1,2048,1024]{2,1,0:T(8,128)(2,1)S(1)}, bf16[1,2048,1024]{2,1,0:T(8,128)(2,1)}, u32[]{:S(2)}) copy-start(bf16[1,2048,1024]{2,1,0:T(8,128)(2,1)} %param.16) | copy-start | bytes 12582916
  83.9 9.5 %copy-start.6 = (bf16[1024,2048]{1,0:T(8,128)(2,1)S(1)}, bf16[1024,2048]{1,0:T(8,128)(2,1)}, u32[]{:S(2)}) copy-start(bf16[1024,2048]{1,0:T(8,128)(2,1)} %all-gather.5.cloned.1.call-done) | copy-start | bytes 12582916
  99.1 0.7 copy-start.3
  99.1 0.7 copy-start.4
  99.1 178.7 %reduce-scatter.2.cloned.1.call-start = ((), (), s32[]{:S(2)}) async-start(), calls=%async_computation.3 | async-start | bytes 4718592 | tf_op jit(solution)/shard_map/reduce_scatter | solution.py:67
  227.7 50.1 %copy-start.7 = (bf16[128,1024]{1,0:T(8,128)(2,1)S(1)}, bf16[128,1024]{1,0:T(8,128)(2,1)}, u32[]{:S(2)}) copy-start(bf16[128,1024]{1,0:T(8,128)(2,1)} %get-tuple-element.7) | copy-start | bytes 786436
  227.7 50.1 %copy-start.8 = (bf16[128,1024]{1,0:T(8,128)(2,1)S(1)}, bf16[128,1024]{1,0:T(8,128)(2,1)}, u32[]{:S(2)}) copy-start(bf16[128,1024]{1,0:T(8,128)(2,1)} %get-tuple-element.8) | copy-start | bytes 786436
  227.7 58.2 %copy-start.2 = (f32[2048]{0:T(1024)S(1)}, f32[2048]{0:T(1024)}, u32[]{:S(2)}) copy-start(f32[2048]{0:T(1024)} %param.21) | copy-start | bytes 24580
Sparse Core Ops, SparseCore 0:
  8.9 23.9 all-gather.2
  37.0 46.8 all-gather.4
  99.3 118.0 all-reduce.2
  227.8 49.9 reduce-scatter.1
where the time goes:
time: 294 us; the launch traced here: 293 us
  waiting for transfers between devices  221 us (75%)
  matrix products  34.1 us (12%)
  blocking collectives  19 us (6%)
  between operations  13.2 us (4%)
  other arithmetic  4.88 us (2%)
    psum x1, waiting for transfers between devices, per_device(): lax.psum(local_product(expert_input, up_matrix).astype(jnp.bfloat16), 'tp')  103 us
    reduce_scatter x1, waiting for transfers between devices, per_device(): lax.psum_scatter((column * expert_rows.astype(jnp.float32)).astype(jnp.bf...  50.1 us
    all_gather x1, waiting for transfers between devices, per_device(): expert_input = lax.all_gather(normed_block, 'ep', axis=0, tiled=True)  41.6 us
    dot_general x6, matrix products, local_product(): return jnp.dot(source, matrix, preferred_element_type=jnp.float32)  34.1 us
    all_gather x1, waiting for transfers between devices, per_device(): full_rows = lax.all_gather(tokens, 'tp', axis=1, tiled=True)  25.6 us
    all_gather x1, blocking collectives, per_device(): table_all = lax.all_gather(weight_table, 'ep', axis=0, tiled=True)  14.1 us
  transfers between devices with their start and end apart: 4, of which 4 were waited for; matrix products, arithmetic and copies ran while one was open for 2% of the time, Pallas kernels for 0%

commit v1 on v0

--- a/solution.py
+++ b/solution.py
@@ -42,8 +42,13 @@
         jnp.float32
     )
     weight_table = jnp.sum(route_weights[:, :, None] * choose, axis=1)
-    expert_input = lax.all_gather(normed_block, "ep", axis=0, tiled=True)
-    table_all = lax.all_gather(weight_table, "ep", axis=0, tiled=True)
+    expert_input, table_all = jnp.split(
+        lax.all_gather(
+            jnp.concatenate([normed_block, weight_table], axis=1), "ep", axis=0, tiled=True
+        ),
+        [normed_block.shape[1]],
+        axis=1,
+    )
     summed = (
         lax.psum(local_product(expert_input, gate_matrix).astype(jnp.bfloat16), "tp").astype(
             jnp.float32

time: 294 us -> 334 us (1.14)
  waiting for transfers between devices: 221 us -> 273 us
  blocking collectives: 19 us -> 4.93 us
    all_gather x1, waiting for transfers between devices: 41.6 us -> 81.3 us  [per_device(): lax.all_gather(jnp.concatenate([normed_block, weight_table], axis=1), 'ep...]
    all_gather x1 -> x0, blocking collectives: 14.1 us -> none  [per_device(): table_all = lax.all_gather(weight_table, 'ep', axis=0, tiled=True)]
    psum x1, waiting for transfers between devices: 103 us -> 117 us  [per_device(): lax.psum(local_product(expert_input, up_matrix).astype(jnp.bfloat16), 'tp')]
where the time goes in v1:
time: 334 us
  waiting for transfers between devices  273 us (82%)
  matrix products  34.9 us (10%)
  between operations  13.2 us (4%)
  other arithmetic  5.9 us (2%)
  blocking collectives  4.93 us (1%)
    psum x1, waiting for transfers between devices, per_device(): lax.psum(local_product(expert_input, up_matrix).astype(jnp.bfloat16), 'tp')  117 us
    all_gather x1, waiting for transfers between devices, per_device(): lax.all_gather(jnp.concatenate([normed_block, weight_table], axis=1), 'ep...  81.3 us
    reduce_scatter x1, waiting for transfers between devices, per_device(): lax.psum_scatter((column * expert_rows.astype(jnp.float32)).astype(jnp.bf...  50.1 us
    dot_general x6, matrix products, local_product(): return jnp.dot(source, matrix, preferred_element_type=jnp.float32)  34.9 us
    all_gather x1, waiting for transfers between devices, per_device(): full_rows = lax.all_gather(tokens, 'tp', axis=1, tiled=True)  24.8 us
  transfers between devices with their start and end apart: 4, of which 4 were waited for; matrix products, arithmetic and copies ran while one was open for 2% of the time, Pallas kernels for 0%

profile of v1, /device:TPU:0, one launch (start us, length us, event | category | flops | bytes accessed | tf_op | source)
XLA Modules:
  0.0 333.8 jit_solution(4524409115692423998)
XLA Ops:
  6.5 0.0 all-gather.3.cloned.1.call-start
  6.5 0.7 all-gather.3.cloned.1.call-update
  7.3 0.0 all-gather.5.cloned.1.call-start
  7.3 0.7 select_reduce_fusion
  8.0 0.1 copy.16
  8.1 0.0 dynamic-slice-start
  8.1 24.8 %all-gather.3.cloned.1.call-done = bf16[128,4096]{1,0:T(8,128)(2,1)} async-done(((bf16[128,2048]{1,0:T(8,128)(2,1)}), bf16[128,4096]{1,0:T(8,128)(2,1)}) %all-gather.3.cloned.1.call-update) | async-done | bytes 1048592 | tf_op jit(solution)/shard_map/all_gather | solution.py:29
  32.9 1.5 multiply_reduce_fusion
  34.4 1.4 convert_element_type.55
  35.9 0.0 dynamic-slice-done
  35.9 0.2 fusion.38
  36.1 1.1 pad_maximum_fusion
  37.2 0.0 all-gather.5.cloned.1.call-update
  37.2 0.0 all-reduce.3.cloned.1.call-start
  37.2 0.0 copy-start
  37.2 3.8 %convolution_convert_fusion.1 = bf16[128,1024]{1,0:T(8,128)(2,1)} fusion(bf16[128,2048]{1,0:T(8,128)(2,1)S(1)} %get-tuple-element.10, bf16[2048,1024]{1,0:T(8,128)(2,1)} %param.18), kind=kOutput, calls=%fused_computation.22 | convolution fusion | flops 537001984 | bytes 4980736 | tf_op jit(solution)/shard_map/dot_general | solution.py:10
  41.0 0.0 copy-done
  41.0 1.4 convolution_convert_fusion
  42.5 81.3 %all-gather.5.cloned.1.call-done = f32[1024,2056]{1,0:T(8,128)} async-done(((f32[128,2056]{1,0:T(8,128)}), f32[1024,2056]{1,0:T(8,128)}) %all-gather.5.cloned.1.call-update) | async-done | bytes 8421392 | tf_op jit(solution)/shard_map/all_gather | solution.py:46
  123.7 0.0 copy-start.1
  123.7 0.0 copy-start.3
  123.7 10.5 %fusion.22 = bf16[1024,1024]{1,0:T(8,128)(2,1)} fusion(bf16[1,2048,1024]{2,1,0:T(8,128)(2,1)} %param.16, f32[1024,2056]{1,0:T(8,128)} %all-gather.5.cloned.1.call-done), kind=kOutput, calls=%fused_computation.20 | convolution fusion | flops 4294967296 | bytes 10485760 | tf_op jit(solution)/shard_map/dot_general | solution.py:10
  134.2 0.0 copy-done.1
  134.2 0.0 copy-done.3
  134.2 5.7 %fusion.17 = bf16[1024,1024]{1,0:T(8,128)(2,1)} fusion(bf16[1,2048,1024]{2,1,0:T(8,128)(2,1)S(1)} %copy-done.3, f32[1024,2056]{1,0:T(8,128)S(1)} %copy-done.1), kind=kOutput, calls=%fused_computation.19 | convolution fusion | flops 4294967296 | bytes 10485760 | tf_op jit(solution)/shard_map/dot_general | solution.py:10
  140.0 0.0 slice-start
  140.0 0.0 all-reduce.3.cloned.1.call-update
  140.0 0.0 reduce-scatter.2.cloned.1.call-start
  140.0 1.0 slice-done
  141.0 0.4 dynamic-slice_reduce_fusion
  141.4 116.5 %all-reduce.3.cloned.1.call-done = (bf16[1024,1024]{1,0:T(8,128)(2,1)}, bf16[1024,1024]{1,0:T(8,128)(2,1)}, bf16[128,1024]{1,0:T(8,128)(2,1)}, bf16[128,1024]{1,0:T(8,128)(2,1)}) async-done(((bf16[1024,1024]{1,0:T(8,128)(2,1)}, bf16[1024,1024]{1,0:T(8,128)(2,1)}, bf16[128,1024]{1,0:T(8,128)(2,1)}, bf16[128,1024]{1,0:T(8,128)(2,1)}), (bf16[1024,1024]{1,0:T(8,128)(2,1)}, bf16[1024,1024]{1,0:T(8,128)(2,1)}, ...) | async-done | bytes 4718608 | tf_op jit(solution)/shard_map/psum | solution.py:56
  257.9 10.2 %multiply_convert_fusion = bf16[1024,2048]{1,0:T(8,128)(2,1)} fusion(f32[1024]{0:T(1024)S(1)} %dynamic-slice_reduce_fusion, bf16[1,1024,2048]{2,1,0:T(8,128)(2,1)} %param.17, bf16[1024,1024]{1,0:T(8,128)(2,1)} %get-tuple-element.5, bf16[1024,1024]{1,0:T(8,128)(2,1)} %get-tuple-element.6), kind=kOutput, calls=%fused_computation | convolution fusion | flops 4311744512 | bytes 12587008 | tf_op jit(solution)/shard_map/dot_general | solution.py:10
  268.1 0.0 copy-start.4
  268.1 0.0 copy-start.5
  268.1 0.0 reduce-scatter.2.cloned.1.call-update
  268.1 0.0 copy-start.2
  268.1 50.1 %reduce-scatter.2.cloned.1.call-done = bf16[128,2048]{1,0:T(8,128)(2,1)} async-done(((bf16[1024,2048]{1,0:T(8,128)(2,1)}), bf16[128,2048]{1,0:T(8,128)(2,1)}) %reduce-scatter.2.cloned.1.call-update) | async-done | bytes 524304 | tf_op jit(solution)/shard_map/reduce_scatter | solution.py:72
  318.2 0.0 copy-done.4
  318.2 0.0 copy-done.5
  318.2 3.2 multiply_reduce_fusion.1
  321.4 4.9 %psum.39 = f32[128,1]{0,1:T(1,128)S(1)} all-reduce(f32[128,1]{0,1:T(1,128)S(1)} %bitcast.23), channel_id=1, replica_groups=mesh['grp'=2,'ep'=8,'tp'=2] {'tp'}, use_global_device_ids=true, to_apply=%region_8.9 | all-reduce | flops 128 | bytes 1024 | tf_op jit(solution)/shard_map/psum | solution.py:79
  326.4 0.0 copy-done.2
  326.4 1.0 multiply_convert_fusion.1
  (2 shorter events, 0.0 us)
Async XLA Ops:
  6.5 26.4 %all-gather.3.cloned.1.call-start = ((), (), s32[]{:S(2)}) async-start(), calls=%async_computation.1 | async-start | bytes 1572864 | tf_op jit(solution)/shard_map/all_gather | solution.py:29
  7.3 116.5 %all-gather.5.cloned.1.call-start = ((), (), s32[]{:S(2)}) async-start(), calls=%async_computation.2 | async-start | bytes 10027008 | tf_op jit(solution)/shard_map/all_gather | solution.py:46
  8.1 27.8 %dynamic-slice-start = ((f32[4096]{0:T(1024)}, s32[]{:T(128)}), f32[2048]{0:T(1024)S(1)}, s32[]{:S(2)}) async-start(f32[4096]{0:T(1024)} %param.14, s32[]{:T(128)} %select_n.6), calls=%async_computation.6 | async-start | bytes 16896 | tf_op jit(solution)/shard_map/dynamic_slice | solution.py:36
  37.2 220.7 %all-reduce.3.cloned.1.call-start = ((), (), s32[]{:S(2)}) async-start(), calls=%async_computation.4 | async-start | bytes 9437184 | tf_op jit(solution)/shard_map/psum | solution.py:56
  37.2 3.8 %copy-start = (bf16[2048,1024]{1,0:T(8,128)(2,1)S(1)}, bf16[2048,1024]{1,0:T(8,128)(2,1)}, u32[]{:S(2)}) copy-start(bf16[2048,1024]{1,0:T(8,128)(2,1)} %param.19) | copy-start | bytes 12582916
  123.7 10.5 %copy-start.1 = (f32[1024,2056]{1,0:T(8,128)S(1)}, f32[1024,2056]{1,0:T(8,128)}, u32[]{:S(2)}) copy-start(f32[1024,2056]{1,0:T(8,128)} %all-gather.5.cloned.1.call-done) | copy-start | bytes 25264132
  123.7 10.5 %copy-start.3 = (bf16[1,2048,1024]{2,1,0:T(8,128)(2,1)S(1)}, bf16[1,2048,1024]{2,1,0:T(8,128)(2,1)}, u32[]{:S(2)}) copy-start(bf16[1,2048,1024]{2,1,0:T(8,128)(2,1)} %param.15) | copy-start | bytes 12582916
  140.0 1.0 slice-start
  140.0 178.2 %reduce-scatter.2.cloned.1.call-start = ((), (), s32[]{:S(2)}) async-start(), calls=%async_computation.3 | async-start | bytes 4718592 | tf_op jit(solution)/shard_map/reduce_scatter | solution.py:72
  268.1 50.1 %copy-start.4 = (bf16[128,1024]{1,0:T(8,128)(2,1)S(1)}, bf16[128,1024]{1,0:T(8,128)(2,1)}, u32[]{:S(2)}) copy-start(bf16[128,1024]{1,0:T(8,128)(2,1)} %get-tuple-element.7) | copy-start | bytes 786436
  268.1 50.1 %copy-start.5 = (bf16[128,1024]{1,0:T(8,128)(2,1)S(1)}, bf16[128,1024]{1,0:T(8,128)(2,1)}, u32[]{:S(2)}) copy-start(bf16[128,1024]{1,0:T(8,128)(2,1)} %get-tuple-element.8) | copy-start | bytes 786436
  268.1 58.2 %copy-start.2 = (f32[2048]{0:T(1024)S(1)}, f32[2048]{0:T(1024)}, u32[]{:S(2)}) copy-start(f32[2048]{0:T(1024)} %param.21) | copy-start | bytes 24580
Sparse Core Ops, SparseCore 0:
  8.9 23.9 all-gather.2
  37.3 86.3 all-gather.4
  140.1 117.7 all-reduce.2
  268.2 49.9 reduce-scatter.1
